TPU v7x, 32 devices: a whole 2x2x4 slice. The times are simulated.
32 devices in a mesh: ep: 8 (over z, core), tp: 4 (over y, x).
Axes of the slice: x: 2, y: 2, z: 4, core: 2. Of those that a mesh axis runs over, the one named last changes fastest.
Arguments:
- gate_out: bfloat16 [2048, 1024], P('ep', 'tp'), may hold values from -6 to 6
- gate_in: bfloat16 [2048, 1024], P('ep', 'tp'), may hold values from -6 to 6
- conv_values: bfloat16 [2048, 1024], P('ep', 'tp'), may hold values from -6 to 6
- conv_taps: float32 [3, 1024], P(None, 'tp'), may hold values from -3 to 3
- mixer_proj: bfloat16 [1024, 2048], P('tp'), may hold values from -0.25 to 0.25
- expert_in: bfloat16 [2048, 2048], P('ep'), may hold values from -6 to 6
- norm_gain: float32 [2048], replicated, may hold values from 0.1 to 1.9
- route_ids: int32 [2048, 2], P('ep'), may hold values from 0 to 7, all different within a row; in each aligned block of 256 rows (0 to 255, 256 to 511, ...) at most 86 rows name the same one
- route_scores: float32 [2048, 2], P('ep'), may hold values from 0.1 to 1
- gate_proj: bfloat16 [8, 2048, 4096], P('ep', None, 'tp'), may hold values from -0.125 to 0.125
- up_proj: bfloat16 [8, 2048, 4096], P('ep', None, 'tp'), may hold values from -0.125 to 0.125
- down_proj: bfloat16 [8, 4096, 2048], P('ep', 'tp'), may hold values from -0.125 to 0.125
Outputs:
- mixed: bfloat16 [2048, 2048], P('ep', 'tp')
- expert_mix: bfloat16 [2048, 2048], P('ep', 'tp')
Inputs may be any that keep to these rules, and one draw needn't show every extreme that they name: `route_ids`: each row names 2 different experts. Within each aligned block of 256 rows (the rows of one device of ep) no expert is named by more than 86 rows, and in some block an expert is named by exactly 86 rows.
All inputs are finite; a program needn't handle non-finite values.
Results may differ from a plain program's by a relative error of at most 0.015.
Values may be sent and summed in bfloat16 or wider, within the bound.
A program may use at most 64 MiB of HBM per device.

v0:
```python
import jax
import jax.numpy as jnp
from jax import lax
from jax.sharding import PartitionSpec as P


def shifted(block, axis, distance):
    devices = range(lax.axis_size(axis))
    route = [(i - distance, i) for i in devices if i - distance in devices]
    return lax.ppermute(block, axis, route)


def slot_table(route_ids, experts_total, capacity):
    pairs = route_ids.reshape(-1)
    onehot = (pairs[:, None] == jnp.arange(experts_total, dtype=jnp.int32)[None, :]).astype(
        jnp.int32
    )
    before = jnp.cumsum(onehot, axis=0) - onehot
    ranking = jnp.sum(before * onehot, axis=1)
    return (pairs * capacity + ranking).reshape(route_ids.shape)


def shards(
    gate_out,
    gate_in,
    conv_values,
    conv_taps,
    mixer_proj,
    expert_in,
    norm_gain,
    route_ids,
    route_scores,
    gate_proj,
    up_proj,
    down_proj,
):
    product = gate_in.astype(jnp.float32) * conv_values.astype(jnp.float32)
    seq_len = product.shape[0]
    tap_count = conv_taps.shape[0]
    earlier = shifted(product[seq_len - (tap_count - 1) :], "ep", 1)
    padded = jnp.concatenate([earlier, product], axis=0)
    convolved = conv_taps[0] * padded[0:seq_len]
    for offset in range(1, tap_count):
        convolved = convolved + conv_taps[offset] * padded[offset : offset + seq_len]
    branch = (gate_out.astype(jnp.float32) * convolved).astype(jnp.bfloat16)
    partial_mix = jnp.dot(branch, mixer_proj, preferred_element_type=jnp.float32)
    mixed = lax.psum_scatter(
        partial_mix.astype(jnp.bfloat16), "tp", scatter_dimension=1, tiled=True
    )
    rows_wide = expert_in.astype(jnp.float32)
    scaling = lax.rsqrt(jnp.mean(rows_wide * rows_wide, axis=1, keepdims=True) + 1e-06)
    normed = (rows_wide * scaling * norm_gain).astype(jnp.bfloat16)
    token_count = expert_in.shape[0]
    choose_count = route_ids.shape[1]
    model_width = expert_in.shape[1]
    ep_count = lax.axis_size("ep")
    local_experts = gate_proj.shape[0]
    experts_total = ep_count * local_experts
    capacity = max(
        2, (4 * token_count * choose_count + 3 * experts_total - 1) // (3 * experts_total)
    )
    slot_count = experts_total * capacity
    slots = slot_table(route_ids, experts_total, capacity)
    hits = slots[None, :, :] == jnp.arange(slot_count, dtype=jnp.int32)[:, None, None]
    dispatch = jnp.sum(hits.astype(jnp.int32), axis=2).astype(jnp.bfloat16)
    column_count = model_width // lax.axis_size("tp")
    own_columns = lax.dynamic_slice_in_dim(
        normed, lax.axis_index("tp") * column_count, column_count, 1
    )
    sent = jnp.dot(dispatch, own_columns, preferred_element_type=jnp.float32).astype(jnp.bfloat16)
    arrived = lax.all_to_all(sent, "ep", split_axis=0, concat_axis=0, tiled=True)
    piece = lax.all_gather(arrived, "tp", axis=1, tiled=True)
    grouped_piece = piece.reshape(ep_count, local_experts, capacity, piece.shape[1])
    gate_part = jnp.einsum(
        "secd,edf->secf", grouped_piece, gate_proj, preferred_element_type=jnp.float32
    )
    up_part = jnp.einsum(
        "secd,edf->secf", grouped_piece, up_proj, preferred_element_type=jnp.float32
    )
    hidden = (jax.nn.silu(gate_part) * up_part).astype(jnp.bfloat16)
    partial_out = jnp.einsum(
        "secf,efd->secd", hidden, down_proj, preferred_element_type=jnp.float32
    )
    summed = lax.psum_scatter(
        partial_out.astype(jnp.bfloat16), "tp", scatter_dimension=3, tiled=True
    )
    returned = lax.all_to_all(summed, "ep", split_axis=0, concat_axis=0, tiled=True)
    slot_rows = returned.reshape(slot_count, returned.shape[3])
    picked = jnp.take(slot_rows, slots.reshape(-1), axis=0).reshape(
        token_count, choose_count, slot_rows.shape[1]
    )
    weights = route_scores / jnp.sum(route_scores, axis=1, keepdims=True)
    expert_mix = jnp.sum(weights[:, :, None] * picked.astype(jnp.float32), axis=1).astype(
        jnp.bfloat16
    )
    return (mixed, expert_mix)


def solution(mesh):
    placed = (
        P("ep", "tp"),
        P("ep", "tp"),
        P("ep", "tp"),
        P(None, "tp"),
        P("tp", None),
        P("ep", None),
        P(),
        P("ep", None),
        P("ep", None),
        P("ep", None, "tp"),
        P("ep", None, "tp"),
        P("ep", "tp", None),
    )
    return jax.shard_map(
        shards,
        mesh=mesh,
        in_specs=placed,
        out_specs=(P("ep", "tp"), P("ep", "tp")),
        check_vma=False,
    )
```

profile of v0, /device:TPU:0, one launch (start us, length us, event | category | flops | bytes accessed | tf_op | source)
XLA Modules:
  0.0 187.0 jit_solution(16390596745611525684)
XLA Ops:
  7.2 0.0 copy-start
  7.2 0.0 copy-start.5
  7.2 0.0 copy-start.1
  7.2 0.0 all-gather.2.cloned.1.call-start
  7.2 0.9 copy.33
  8.2 0.1 eq.39
  8.3 0.1 reshape.111
  8.5 2.8 %convert_element_type.67 = f32[256,2048]{1,0:T(8,128)} convert(bf16[256,2048]{1,0:T(8,128)(2,1)} %param.17) | non-fusion elementwise | flops 524288 | bytes 3145728 | tf_op jit(solution)/shard_map/convert_element_type | solution.py:50
  11.3 0.0 copy-done.1
  11.3 0.3 multiply_reduce_fusion
  11.6 1.1 reduce-window.6
  12.8 0.2 slice_reduce_fusion
  13.0 0.1 fusion.41
  13.1 0.1 reduce_sum.51
  13.3 0.1 copy.35
  13.3 0.0 copy-done.5
  13.4 0.3 convert_reduce_fusion
  13.7 0.8 dynamic-slice
  14.4 1.5 convolution_convert_fusion.1
  15.9 0.2 all_to_all.11
  16.1 25.7 %all_to_all.17 = bf16[8,86,512]{2,1,0:T(8,128)(2,1)S(1)} all-to-all(bf16[8,86,512]{2,1,0:T(8,128)(2,1)S(1)} %all_to_all.11), channel_id=1, replica_groups=mesh['ep'=8,'tp'=4] {'ep'}, dimensions={0} | all-to-all | bytes 1409024 | tf_op jit(solution)/shard_map/all_to_all | solution.py:71
  41.8 1.1 all_to_all.13
  42.9 0.0 all-gather.2.cloned.1.call-update
  42.9 0.0 reduce-scatter.5.cloned.1.call-start
  42.9 40.0 %all-gather.2.cloned.1.call-done = bf16[688,2048]{1,0:T(8,128)(2,1)} async-done(((bf16[688,512]{1,0:T(8,128)(2,1)}), bf16[688,2048]{1,0:T(8,128)(2,1)}) %all-gather.2.cloned.1.call-update) | async-done | bytes 2818064 | tf_op jit(solution)/shard_map/all_gather | solution.py:72
  83.0 3.3 %reshape.113 = bf16[8,86,2048]{2,1,0:T(8,128)(2,1)} reshape(bf16[688,2048]{1,0:T(8,128)(2,1)} %all-gather.2.cloned.1.call-done) | data formatting | bytes 5636096 | tf_op jit(solution)/shard_map/reshape.9
  86.3 7.8 %fusion.2 = f32[8,86,1024]{2,1,0:T(8,128)} fusion(bf16[8,86,2048]{2,1,0:T(8,128)(2,1)} %reshape.113, bf16[1,2048,1024]{2,1,0:T(8,128)(2,1)} %param.22), kind=kOutput, calls=%fused_computation.3 | convolution fusion | flops 2885681152 | bytes 9830400 | tf_op jit(solution)/shard_map/secd,edf->secf/dot_general | solution.py:77
  94.1 13.0 %fusion.9 = bf16[8,1,86,2048]{3,2,0,1:T(8,128)(2,1)} fusion(bf16[1,1024,2048]{2,1,0:T(8,128)(2,1)} %param.23, f32[8,86,1024]{2,1,0:T(8,128)} %fusion.2, bf16[8,86,2048]{2,1,0:T(8,128)(2,1)} %reshape.113, bf16[1,2048,1024]{2,1,0:T(8,128)(2,1)} %param.21), kind=kOutput, calls=%fused_computation.8 | convolution fusion | flops 5776998400 | bytes 16842752 | tf_op jit(solution)/shard_map/secf,efd->secd/dot_general | solution.py:81
  107.1 0.0 copy-start.3
  107.1 0.0 copy-start.4
  107.1 0.0 copy-start.7
  107.1 0.0 copy-start.2
  107.1 0.0 reduce-scatter.5.cloned.1.call-update
  107.2 0.0 copy-start.6
  107.2 0.0 reduce-scatter.3.cloned.1.call-start
  107.2 0.8 copy-done.3
  108.0 0.1 copy-done.4
  108.1 1.6 collective-permute-start
  109.7 0.0 copy-done.7
  109.7 0.8 collective-permute-done
  110.5 0.0 copy-done
  110.5 0.0 copy-done.2
  110.5 1.4 convolution_convert_fusion
  112.0 0.0 reduce-scatter.3.cloned.1.call-update
  112.0 37.0 %reduce-scatter.5.cloned.1.call-done = bf16[8,1,86,512]{3,2,0,1:T(8,128)(2,1)} async-done(((bf16[8,1,86,2048]{3,2,0,1:T(8,128)(2,1)}), bf16[8,1,86,512]{3,2,0,1:T(8,128)(2,1)}) %reduce-scatter.5.cloned.1.call-update) | async-done | bytes 704528 | tf_op jit(solution)/shard_map/reduce_scatter | solution.py:84
  149.0 4.6 %all-to-all-start.1 = ((bf16[8,1,86,512]{3,2,1,0:T(8,128)(2,1)}), bf16[8,1,86,512]{3,2,1,0:T(8,128)(2,1)S(1)}, u32[]{:S(2)}, u32[]{:S(2)}) async-start(bf16[8,1,86,512]{3,2,1,0:T(8,128)(2,1)} %bitcast.82), calls=%async_computation.3 | async-start | bytes 1441792 | tf_op jit(solution)/shard_map/all_to_all | solution.py:87
  153.7 0.1 copy.38
  153.8 0.1 mul.120
  154.0 0.2 copy.36
  154.1 0.0 copy-done.6
  154.2 0.1 copy.32
  154.4 18.8 %all-to-all-done.1 = bf16[8,1,86,512]{3,2,1,0:T(8,128)(2,1)S(1)} async-done(((bf16[8,1,86,512]{3,2,1,0:T(8,128)(2,1)}), bf16[8,1,86,512]{3,2,1,0:T(8,128)(2,1)S(1)}, u32[]{:S(2)}, u32[]{:S(2)}) %all-to-all-start.1) | async-done | bytes 704544 | tf_op jit(solution)/shard_map/all_to_all | solution.py:87
  173.2 0.2 reshape.118
  173.4 2.0 %gather_fusion = bf16[512,512]{1,0:T(8,128)(2,1)S(1)} fusion(bf16[688,512]{1,0:T(8,128)(2,1)S(1)} %reshape.118, s32[1024]{0:T(1024)S(1)} %pad_clamp_fusion), kind=kCustom, calls=%fused_computation | custom fusion | bytes 1050624 | tf_op jit(solution)/shard_map/jit(_take)/gather | solution.py:89
  175.4 0.2 gather.7
  175.6 2.9 %multiply_reduce_fusion.1 = bf16[256,512]{1,0:T(8,128)(2,1)} fusion(bf16[256,2,512]{2,1,0:T(2,128)(2,1)S(1)} %gather.7, pred[256,2]{1,0:T(8,128)(4,1)S(1)} %copy.36, f32[256,2]{1,0:T(8,128)S(1)} %copy.32), kind=kLoop, calls=%fused_computation.22 | loop fusion | flops 917504 | bytes 788992 | tf_op jit(solution)/shard_map/reduce_sum | solution.py:93
  178.5 2.0 %reduce-scatter.3.cloned.1.call-done = bf16[256,512]{1,0:T(8,128)(2,1)} async-done(((bf16[256,2048]{1,0:T(8,128)(2,1)}), bf16[256,512]{1,0:T(8,128)(2,1)}) %reduce-scatter.3.cloned.1.call-update) | async-done | bytes 262160 | tf_op jit(solution)/shard_map/reduce_scatter | solution.py:47
  (13 shorter events, 0.1 us)
Async XLA Ops:
  7.2 103.4 %copy-start = (bf16[256,2048]{1,0:T(8,128)(2,1)S(1)}, bf16[256,2048]{1,0:T(8,128)(2,1)}, u32[]{:S(2)}) copy-start(bf16[256,2048]{1,0:T(8,128)(2,1)} %param.16) | copy-start | bytes 3145732
  7.2 6.2 %copy-start.5 = (s32[256,2]{0,1:T(2,128)S(1)}, s32[256,2]{0,1:T(2,128)}, u32[]{:S(2)}) copy-start(s32[256,2]{0,1:T(2,128)} %param.19) | copy-start | bytes 6148
  7.2 4.1 %copy-start.1 = (bf16[256,2048]{1,0:T(8,128)(2,1)S(1)}, bf16[256,2048]{1,0:T(8,128)(2,1)}, u32[]{:S(2)}) copy-start(bf16[256,2048]{1,0:T(8,128)(2,1)} %param.17) | copy-start | bytes 3145732
  7.2 75.8 %all-gather.2.cloned.1.call-start = ((), (), s32[]{:S(2)}) async-start(), calls=%async_computation.5 | async-start | bytes 3522560 | tf_op jit(solution)/shard_map/all_gather | solution.py:72
  42.9 106.2 %reduce-scatter.5.cloned.1.call-start = ((), (), s32[]{:S(2)}) async-start(), calls=%async_computation.6 | async-start | bytes 3604480 | tf_op jit(solution)/shard_map/reduce_scatter | solution.py:84
  107.1 0.9 copy-start.3
  107.1 1.0 copy-start.4
  107.1 2.6 %copy-start.7 = (f32[3,256]{1,0:T(4,128)S(1)}, f32[3,256]{1,0:T(4,128)}, u32[]{:S(2)}) copy-start(f32[3,256]{1,0:T(4,128)} %param.15) | copy-start | bytes 9220
  107.1 3.4 %copy-start.2 = (bf16[256,256]{1,0:T(8,128)(2,1)S(1)}, bf16[256,256]{1,0:T(8,128)(2,1)}, u32[]{:S(2)}) copy-start(bf16[256,256]{1,0:T(8,128)(2,1)} %param.12) | copy-start | bytes 393220
  107.2 47.0 %copy-start.6 = (f32[256,2]{0,1:T(2,128)S(1)}, f32[256,2]{0,1:T(2,128)}, u32[]{:S(2)}) copy-start(f32[256,2]{0,1:T(2,128)} %param.20) | copy-start | bytes 6148
  107.2 73.3 %reduce-scatter.3.cloned.1.call-start = ((), (), s32[]{:S(2)}) async-start(), calls=%async_computation.4 | async-start | bytes 1310720 | tf_op jit(solution)/shard_map/reduce_scatter | solution.py:47
  108.1 2.4 %collective-permute-start = (f32[2,256]{1,0:T(2,128)S(1)}, f32[2,256]{1,0:T(2,128)S(1)}, u32[]{:S(2)}, u32[]{:S(2)}) collective-permute-start(f32[2,256]{1,0:T(2,128)S(1)} %slice.34), channel_id=1, source_target_pairs={{0,4},{4,8},{8,12},{12,16},{16,20},{20,24},{24,28},{1,5},{5,9},{9,... | collective-permute-start | bytes 6152 | tf_op jit(solution)/shard_map/ppermute | solution.py:10
  149.0 24.1 %all-to-all-start.1 = ((bf16[8,1,86,512]{3,2,1,0:T(8,128)(2,1)}), bf16[8,1,86,512]{3,2,1,0:T(8,128)(2,1)S(1)}, u32[]{:S(2)}, u32[]{:S(2)}) async-start(bf16[8,1,86,512]{3,2,1,0:T(8,128)(2,1)} %bitcast.82), calls=%async_computation.3 | async-start | bytes 1441792 | tf_op jit(solution)/shard_map/all_to_all | solution.py:87
Sparse Core Ops, SparseCore 0:
  43.0 39.9 all-gather.1
  107.3 41.7 reduce-scatter.4
  152.5 27.9 reduce-scatter.2
where the time goes:
time: 187 us
  waiting for transfers between devices  98.8 us (53%)
  blocking collectives  25.7 us (14%)
  matrix products  23.7 us (13%)
  between operations  14 us (7%)
  local copies, waits for them, and re-layouts  10.9 us (6%)
  other arithmetic  7.69 us (4%)
  starting transfers between devices  6.31 us (3%)
    all_gather x1, waiting for transfers between devices, shards(): piece = lax.all_gather(arrived, 'tp', axis=1, tiled=True)  40 us
    reduce_scatter x1, waiting for transfers between devices, shards(): lax.psum_scatter(partial_out.astype(jnp.bfloat16), 'tp', scatter_dimensio...  37 us
    all_to_all x1, blocking collectives, shards(): lax.all_to_all(sent, 'ep', split_axis=0, concat_axis=0, tiled=True)  25.7 us
    all_to_all x1, waiting for transfers between devices, shards(): lax.all_to_all(summed, 'ep', split_axis=0, concat_axis=0, tiled=True)  18.8 us
    dot_general x1, matrix products, shards(): jnp.einsum('secf,efd->secd', hidden, down_proj, preferred_element_type=jn...  13 us
    dot_general x1, matrix products, shards(): jnp.einsum('secd,edf->secf', grouped_piece, up_proj, preferred_element_ty...  7.78 us
    all_to_all x1, starting transfers between devices, shards(): lax.all_to_all(summed, 'ep', split_axis=0, concat_axis=0, tiled=True)  4.61 us
  transfers between devices with their start and end apart: 5, of which 5 were waited for; matrix products, arithmetic and copies ran while one was open for 4% of the time, Pallas kernels for 0%

commit v1 on v0

--- a/solution.py
+++ b/solution.py
@@ -69,7 +69,7 @@
     )
     sent = jnp.dot(dispatch, own_columns, preferred_element_type=jnp.float32).astype(jnp.bfloat16)
     arrived = lax.all_to_all(sent, "ep", split_axis=0, concat_axis=0, tiled=True)
-    piece = lax.all_gather(arrived, "tp", axis=1, tiled=True)
+    piece = jnp.concatenate(lax.all_gather(arrived, "tp"), axis=1)
     grouped_piece = piece.reshape(ep_count, local_experts, capacity, piece.shape[1])
     gate_part = jnp.einsum(
         "secd,edf->secf", grouped_piece, gate_proj, preferred_element_type=jnp.float32

time: 187 us -> 195 us (1.043)
  local copies, waits for them, and re-layouts: 10.9 us -> 17.9 us
    reshape x0 -> x1, local copies, waits for them, and re-layouts: none -> 5.52 us  [shards(): piece = jnp.concatenate(lax.all_gather(arrived, 'tp'), axis=1)]
where the time goes in v1:
time: 195 us; the launch traced here: 194 us
  waiting for transfers between devices  98.7 us (51%)
  blocking collectives  25.7 us (13%)
  matrix products  23.7 us (12%)
  local copies, waits for them, and re-layouts  17.9 us (9%)
  between operations  14 us (7%)
  other arithmetic  7.69 us (4%)
  starting transfers between devices  6.48 us (3%)
    all_gather x1, waiting for transfers between devices, shards(): piece = jnp.concatenate(lax.all_gather(arrived, 'tp'), axis=1)  40.2 us
    reduce_scatter x1, waiting for transfers between devices, shards(): lax.psum_scatter(partial_out.astype(jnp.bfloat16), 'tp', scatter_dimensio...  37 us
    all_to_all x1, blocking collectives, shards(): lax.all_to_all(sent, 'ep', split_axis=0, concat_axis=0, tiled=True)  25.7 us
    all_to_all x1, waiting for transfers between devices, shards(): lax.all_to_all(summed, 'ep', split_axis=0, concat_axis=0, tiled=True)  18.8 us
    dot_general x1, matrix products, shards(): jnp.einsum('secf,efd->secd', hidden, down_proj, preferred_element_type=jn...  13 us
    dot_general x1, matrix products, shards(): jnp.einsum('secd,edf->secf', grouped_piece, up_proj, preferred_element_ty...  7.78 us
    reshape x1, local copies, waits for them, and re-layouts, shards(): piece = jnp.concatenate(lax.all_gather(arrived, 'tp'), axis=1)  5.52 us
    another operation x2, local copies, waits for them, and re-layouts  4.85 us
  transfers between devices with their start and end apart: 5, of which 5 were waited for; matrix products, arithmetic and copies ran while one was open for 4% of the time, Pallas kernels for 0%

profile of v1, /device:TPU:0, one launch (start us, length us, event | category | flops | bytes accessed | tf_op | source)
XLA Modules:
  0.0 194.2 jit_solution(4127801606866030137)
XLA Ops:
  7.2 0.0 copy-start
  7.2 0.0 copy-start.5
  7.2 0.0 copy-start.1
  7.2 0.0 all-gather.2.cloned.1.call-start
  7.2 0.9 copy.37
  8.2 0.1 eq.39
  8.3 0.1 reshape.114
  8.5 2.8 %convert_element_type.67 = f32[256,2048]{1,0:T(8,128)} convert(bf16[256,2048]{1,0:T(8,128)(2,1)} %param.17) | non-fusion elementwise | flops 524288 | bytes 3145728 | tf_op jit(solution)/shard_map/convert_element_type | solution.py:50
  11.3 0.0 copy-done.1
  11.3 0.3 multiply_reduce_fusion
  11.6 1.1 reduce-window.6
  12.8 0.2 slice_reduce_fusion
  13.0 0.1 fusion.41
  13.1 0.1 reduce_sum.51
  13.3 0.1 copy.39
  13.3 0.0 copy-done.5
  13.4 0.3 convert_reduce_fusion
  13.7 0.8 dynamic-slice
  14.4 1.5 convolution_convert_fusion.1
  15.9 0.2 all_to_all.9
  16.1 25.7 %all_to_all.14 = bf16[8,86,512]{2,1,0:T(8,128)(2,1)S(1)} all-to-all(bf16[8,86,512]{2,1,0:T(8,128)(2,1)S(1)} %all_to_all.9), channel_id=1, replica_groups=mesh['ep'=8,'tp'=4] {'ep'}, dimensions={0} | all-to-all | bytes 1409024 | tf_op jit(solution)/shard_map/all_to_all | solution.py:71
  41.8 1.1 all_gather.6
  42.9 0.0 all-gather.2.cloned.1.call-update
  42.9 0.0 reduce-scatter.5.cloned.1.call-start
  42.9 40.2 %all-gather.2.cloned.1.call-done = bf16[4,688,512]{2,1,0:T(8,128)(2,1)} async-done(((bf16[1,688,512]{2,1,0:T(8,128)(2,1)}), bf16[4,688,512]{2,1,0:T(8,128)(2,1)}) %all-gather.2.cloned.1.call-update) | async-done | bytes 2818064 | tf_op jit(solution)/shard_map/all_gather | solution.py:72
  83.1 5.5 %copy.41 = bf16[688,4,512]{2,1,0:T(4,128)(2,1)} copy(bf16[688,4,512]{2,0,1:T(8,128)(2,1)} %bitcast.83) | data formatting | bytes 5636096 | tf_op jit(solution)/shard_map/reshape | solution.py:72
  88.6 4.8 %reshape.117 = bf16[8,86,2048]{2,1,0:T(8,128)(2,1)} reshape(bf16[688,4,512]{2,1,0:T(4,128)(2,1)} %copy.41) | data formatting | bytes 5636096 | tf_op jit(solution)/shard_map/reshape.9
  93.5 7.8 %fusion.2 = f32[8,86,1024]{2,1,0:T(8,128)} fusion(bf16[8,86,2048]{2,1,0:T(8,128)(2,1)} %reshape.117, bf16[1,2048,1024]{2,1,0:T(8,128)(2,1)} %param.22), kind=kOutput, calls=%fused_computation.3 | convolution fusion | flops 2885681152 | bytes 9830400 | tf_op jit(solution)/shard_map/secd,edf->secf/dot_general | solution.py:77
  101.2 13.0 %fusion.9 = bf16[8,1,86,2048]{3,2,0,1:T(8,128)(2,1)} fusion(bf16[1,1024,2048]{2,1,0:T(8,128)(2,1)} %param.23, f32[8,86,1024]{2,1,0:T(8,128)} %fusion.2, bf16[8,86,2048]{2,1,0:T(8,128)(2,1)} %reshape.117, bf16[1,2048,1024]{2,1,0:T(8,128)(2,1)} %param.21), kind=kOutput, calls=%fused_computation.8 | convolution fusion | flops 5776998400 | bytes 16842752 | tf_op jit(solution)/shard_map/secf,efd->secd/dot_general | solution.py:81
  114.3 0.0 copy-start.3
  114.3 0.0 copy-start.4
  114.3 0.0 copy-start.7
  114.3 0.0 copy-start.2
  114.3 0.0 reduce-scatter.5.cloned.1.call-update
  114.3 0.0 copy-start.6
  114.3 0.0 reduce-scatter.3.cloned.1.call-start
  114.4 0.8 copy-done.3
  115.2 0.1 copy-done.4
  115.3 1.8 collective-permute-start
  117.1 0.0 copy-done.7
  117.1 0.6 collective-permute-done
  117.7 0.0 copy-done
  117.7 0.0 copy-done.2
  117.7 1.4 convolution_convert_fusion
  119.1 0.0 reduce-scatter.3.cloned.1.call-update
  119.2 37.0 %reduce-scatter.5.cloned.1.call-done = bf16[8,1,86,512]{3,2,0,1:T(8,128)(2,1)} async-done(((bf16[8,1,86,2048]{3,2,0,1:T(8,128)(2,1)}), bf16[8,1,86,512]{3,2,0,1:T(8,128)(2,1)}) %reduce-scatter.5.cloned.1.call-update) | async-done | bytes 704528 | tf_op jit(solution)/shard_map/reduce_scatter | solution.py:84
  156.2 4.6 %all-to-all-start.1 = ((bf16[8,1,86,512]{3,2,1,0:T(8,128)(2,1)}), bf16[8,1,86,512]{3,2,1,0:T(8,128)(2,1)S(1)}, u32[]{:S(2)}, u32[]{:S(2)}) async-start(bf16[8,1,86,512]{3,2,1,0:T(8,128)(2,1)} %bitcast.84), calls=%async_computation.3 | async-start | bytes 1441792 | tf_op jit(solution)/shard_map/all_to_all | solution.py:87
  160.8 0.1 copy.43
  161.0 0.1 mul.120
  161.1 0.2 copy.40
  161.3 0.0 copy-done.6
  161.3 0.1 copy.36
  161.5 18.8 %all-to-all-done.1 = bf16[8,1,86,512]{3,2,1,0:T(8,128)(2,1)S(1)} async-done(((bf16[8,1,86,512]{3,2,1,0:T(8,128)(2,1)}), bf16[8,1,86,512]{3,2,1,0:T(8,128)(2,1)S(1)}, u32[]{:S(2)}, u32[]{:S(2)}) %all-to-all-start.1) | async-done | bytes 704544 | tf_op jit(solution)/shard_map/all_to_all | solution.py:87
  180.3 0.2 reshape.122
  180.5 2.0 %gather_fusion = bf16[512,512]{1,0:T(8,128)(2,1)S(1)} fusion(bf16[688,512]{1,0:T(8,128)(2,1)S(1)} %reshape.122, s32[1024]{0:T(1024)S(1)} %pad_clamp_fusion), kind=kCustom, calls=%fused_computation | custom fusion | bytes 1050624 | tf_op jit(solution)/shard_map/jit(_take)/gather | solution.py:89
  182.5 0.2 gather.7
  182.7 2.9 %multiply_reduce_fusion.1 = bf16[256,512]{1,0:T(8,128)(2,1)} fusion(bf16[256,2,512]{2,1,0:T(2,128)(2,1)S(1)} %gather.7, pred[256,2]{1,0:T(8,128)(4,1)S(1)} %copy.40, f32[256,2]{1,0:T(8,128)S(1)} %copy.36), kind=kLoop, calls=%fused_computation.22 | loop fusion | flops 917504 | bytes 788992 | tf_op jit(solution)/shard_map/reduce_sum | solution.py:93
  185.6 2.0 %reduce-scatter.3.cloned.1.call-done = bf16[256,512]{1,0:T(8,128)(2,1)} async-done(((bf16[256,2048]{1,0:T(8,128)(2,1)}), bf16[256,512]{1,0:T(8,128)(2,1)}) %reduce-scatter.3.cloned.1.call-update) | async-done | bytes 262160 | tf_op jit(solution)/shard_map/reduce_scatter | solution.py:47
  (13 shorter events, 0.1 us)
Async XLA Ops:
  7.2 110.5 %copy-start = (bf16[256,2048]{1,0:T(8,128)(2,1)S(1)}, bf16[256,2048]{1,0:T(8,128)(2,1)}, u32[]{:S(2)}) copy-start(bf16[256,2048]{1,0:T(8,128)(2,1)} %param.16) | copy-start | bytes 3145732
  7.2 6.2 %copy-start.5 = (s32[256,2]{0,1:T(2,128)S(1)}, s32[256,2]{0,1:T(2,128)}, u32[]{:S(2)}) copy-start(s32[256,2]{0,1:T(2,128)} %param.19) | copy-start | bytes 6148
  7.2 4.1 %copy-start.1 = (bf16[256,2048]{1,0:T(8,128)(2,1)S(1)}, bf16[256,2048]{1,0:T(8,128)(2,1)}, u32[]{:S(2)}) copy-start(bf16[256,2048]{1,0:T(8,128)(2,1)} %param.17) | copy-start | bytes 3145732
  7.2 75.9 %all-gather.2.cloned.1.call-start = ((), (), s32[]{:S(2)}) async-start(), calls=%async_computation.5 | async-start | bytes 3522560 | tf_op jit(solution)/shard_map/all_gather | solution.py:72
  42.9 113.3 %reduce-scatter.5.cloned.1.call-start = ((), (), s32[]{:S(2)}) async-start(), calls=%async_computation.6 | async-start | bytes 3604480 | tf_op jit(solution)/shard_map/reduce_scatter | solution.py:84
  114.3 0.9 copy-start.3
  114.3 1.0 copy-start.4
  114.3 2.8 %copy-start.7 = (f32[3,256]{1,0:T(4,128)S(1)}, f32[3,256]{1,0:T(4,128)}, u32[]{:S(2)}) copy-start(f32[3,256]{1,0:T(4,128)} %param.15) | copy-start | bytes 9220
  114.3 3.4 %copy-start.2 = (bf16[256,256]{1,0:T(8,128)(2,1)S(1)}, bf16[256,256]{1,0:T(8,128)(2,1)}, u32[]{:S(2)}) copy-start(bf16[256,256]{1,0:T(8,128)(2,1)} %param.12) | copy-start | bytes 393220
  114.3 47.0 %copy-start.6 = (f32[256,2]{0,1:T(2,128)S(1)}, f32[256,2]{0,1:T(2,128)}, u32[]{:S(2)}) copy-start(f32[256,2]{0,1:T(2,128)} %param.20) | copy-start | bytes 6148
  114.3 73.3 %reduce-scatter.3.cloned.1.call-start = ((), (), s32[]{:S(2)}) async-start(), calls=%async_computation.4 | async-start | bytes 1310720 | tf_op jit(solution)/shard_map/reduce_scatter | solution.py:47
  115.3 2.4 %collective-permute-start = (f32[2,256]{1,0:T(2,128)S(1)}, f32[2,256]{1,0:T(2,128)S(1)}, u32[]{:S(2)}, u32[]{:S(2)}) collective-permute-start(f32[2,256]{1,0:T(2,128)S(1)} %slice.34), channel_id=1, source_target_pairs={{0,4},{4,8},{8,12},{12,16},{16,20},{20,24},{24,28},{1,5},{5,9},{9,... | collective-permute-start | bytes 6152 | tf_op jit(solution)/shard_map/ppermute | solution.py:10
  156.2 24.1 %all-to-all-start.1 = ((bf16[8,1,86,512]{3,2,1,0:T(8,128)(2,1)}), bf16[8,1,86,512]{3,2,1,0:T(8,128)(2,1)S(1)}, u32[]{:S(2)}, u32[]{:S(2)}) async-start(bf16[8,1,86,512]{3,2,1,0:T(8,128)(2,1)} %bitcast.84), calls=%async_computation.3 | async-start | bytes 1441792 | tf_op jit(solution)/shard_map/all_to_all | solution.py:87
Sparse Core Ops, SparseCore 0:
  43.0 40.0 all-gather.1
  114.4 41.7 reduce-scatter.4
  159.7 27.9 reduce-scatter.2
